TPU v7x, 32 devices: a whole 2x2x4 slice. The times are simulated.
32 devices in a mesh: sp: 8 (over z, x), tp: 4 (over y, core).
Axes of the slice: x: 2, y: 2, z: 4, core: 2. Of those that a mesh axis runs over, the one named last changes fastest.
Arguments:
- tokens: bfloat16 [8, 80, 4096], P(None, 'sp', 'tp'), may hold values from -6 to 6
- latent_down_weight: bfloat16 [4096, 512], replicated, may hold values from -0.09375 to 0.09375
- w_rope_key: bfloat16 [4096, 64], replicated, may hold values from -0.09375 to 0.09375
- latent_norm_gain: float32 [512], replicated, may hold values from 0.1 to 1.9
- key_up_weight: bfloat16 [512, 4096], P(None, 'tp'), may hold values from -0.25 to 0.25
- value_up_weight: bfloat16 [512, 4096], P(None, 'tp'), may hold values from -0.25 to 0.25
- cached_latent_rows: bfloat16 [8, 32768, 512], P('sp', 'tp'), may hold values from -6 to 6
- past_rope: bfloat16 [8, 32768, 64], P('sp', 'tp'), may hold values from -6 to 6
- query_nope: bfloat16 [8, 4096], P('sp', 'tp'), may hold values from -8 to 8
- query_rope: bfloat16 [8, 2048], P('sp', 'tp'), may hold values from -300 to 300
Outputs:
- new_keys: bfloat16 [8, 80, 4096], P('sp', None, 'tp')
- new_values: bfloat16 [8, 80, 4096], P('sp', None, 'tp')
- new_rope: bfloat16 [8, 80, 64], P('sp')
- attended: bfloat16 [8, 4096], P('sp', 'tp')
All inputs are finite; a program needn't handle non-finite values.
Results may differ from a plain program's by a relative error of at most 0.0085.
Values may be sent and summed in bfloat16 or wider, within the bound.
A program may use at most 64 MiB of HBM per device.

v0:
```python
import jax
import jax.numpy as jnp
from jax import lax
from jax.sharding import PartitionSpec as P

PLAIN_KEY_WIDTH = 128
ROPE = 64
VALUE_WIDTH = 128
PAST_POSITIONS = 32768


epsilon = 1e-06
rope_theta = 10000.0


def combined_all(part, axis, combine):
    gathered = jax.tree.map(lambda a: lax.all_gather(a, axis), part)

    def take(source):
        return jax.tree.map(lambda a: lax.dynamic_index_in_dim(a, source, 0, False), gathered)

    return lax.fori_loop(
        1, lax.axis_size(axis), lambda source, state: combine(state, take(source)), take(0)
    )


def rotate(values, positions):
    halfway = values.shape[-1] // 2
    frequency = rope_theta ** (-jnp.arange(halfway, dtype=jnp.float32) / halfway)
    angles = positions[:, None] * frequency
    first = values[..., :halfway]
    second = values[..., halfway:]
    return jnp.concatenate(
        [
            first * jnp.cos(angles) - second * jnp.sin(angles),
            first * jnp.sin(angles) + second * jnp.cos(angles),
        ],
        axis=-1,
    )


def combine_parts(first, second):
    highest = jnp.maximum(first[0], second[0])
    scale_first = jnp.exp(first[0] - highest)
    scale_second = jnp.exp(second[0] - highest)
    total = first[1] * scale_first + second[1] * scale_second
    summed = first[2] * scale_first[..., None] + second[2] * scale_second[..., None]
    return (highest, total, summed)


def on_device(
    tokens,
    latent_down_weight,
    w_rope_key,
    latent_norm_gain,
    key_up_weight,
    value_up_weight,
    cached_latent_rows,
    past_rope,
    query_nope,
    query_rope,
):
    rows_here = lax.all_to_all(tokens, "sp", split_axis=0, concat_axis=1, tiled=True)
    prompts, per_seq, features = rows_here.shape
    row_count = prompts * per_seq
    latent_width = latent_down_weight.shape[1]
    turn_width = w_rope_key.shape[1]
    factor = (PLAIN_KEY_WIDTH + ROPE) ** (-0.5)
    fragment = lax.all_gather(rows_here, "tp", axis=2, tiled=True)
    columns = fragment.shape[2]
    flat_rows = fragment.reshape(row_count, columns)
    latent_raw = jnp.dot(flat_rows, latent_down_weight, preferred_element_type=jnp.float32)
    rope_raw = jnp.dot(flat_rows, w_rope_key, preferred_element_type=jnp.float32)
    scale = lax.rsqrt(jnp.mean(latent_raw * latent_raw, axis=-1, keepdims=True) + epsilon)
    latent = (latent_raw * scale * latent_norm_gain).astype(jnp.bfloat16)
    positions = (PAST_POSITIONS + jnp.arange(per_seq)).astype(jnp.float32)
    rope_local = rotate(rope_raw.reshape(prompts, per_seq, turn_width), positions).astype(
        jnp.bfloat16
    )
    keys_local = (
        jnp.dot(latent, key_up_weight, preferred_element_type=jnp.float32)
        .astype(jnp.bfloat16)
        .reshape(prompts, per_seq, key_up_weight.shape[1])
    )
    values_local = (
        jnp.dot(latent, value_up_weight, preferred_element_type=jnp.float32)
        .astype(jnp.bfloat16)
        .reshape(prompts, per_seq, value_up_weight.shape[1])
    )
    new_keys, new_values, new_rope = (keys_local, values_local, rope_local)
    owned = query_nope.shape[0]
    heads_local = query_nope.shape[1] // PLAIN_KEY_WIDTH
    query_own = query_nope.reshape(owned, heads_local, PLAIN_KEY_WIDTH)
    turn_own = query_rope.reshape(owned, heads_local, ROPE)
    head_keys = key_up_weight.reshape(latent_width, heads_local, PLAIN_KEY_WIDTH)
    query_latent = jnp.einsum(
        "shd,khd->shk", query_own, head_keys, preferred_element_type=jnp.float32
    ).astype(jnp.bfloat16)
    every_latent, every_turn = (
        lax.all_gather(query_latent, "tp", axis=1, tiled=True),
        lax.all_gather(turn_own, "tp", axis=1, tiled=True),
    )
    past_scores = jnp.einsum(
        "shk,spk->shp", every_latent, cached_latent_rows, preferred_element_type=jnp.float32
    )
    past_scores = (
        past_scores
        + jnp.einsum("shd,spd->shp", every_turn, past_rope, preferred_element_type=jnp.float32)
    ) * factor
    local_peak = jnp.max(past_scores, axis=-1)
    local_weight = jnp.exp(past_scores - local_peak[:, :, None])
    local_total = jnp.sum(local_weight, axis=-1)
    local_latent = jnp.einsum(
        "shp,spk->shk",
        local_weight.astype(jnp.bfloat16),
        cached_latent_rows,
        preferred_element_type=jnp.float32,
    )
    peak_all, total_all, latent_all = combined_all(
        (local_peak, local_total, local_latent), "tp", combine_parts
    )
    start = lax.axis_index("tp") * heads_local
    past_peak = lax.dynamic_slice_in_dim(peak_all, start, heads_local, 1)
    past_total = lax.dynamic_slice_in_dim(total_all, start, heads_local, 1)
    past_sum = lax.dynamic_slice_in_dim(latent_all, start, heads_local, 1)
    fresh = new_keys.shape[1]
    new_scores = jnp.einsum(
        "shd,sphd->shp",
        query_own,
        new_keys.reshape(owned, fresh, heads_local, PLAIN_KEY_WIDTH),
        preferred_element_type=jnp.float32,
    )
    new_scores = (
        new_scores
        + jnp.einsum("shd,spd->shp", turn_own, new_rope, preferred_element_type=jnp.float32)
    ) * factor
    peak = jnp.maximum(past_peak, jnp.max(new_scores, axis=-1))
    past_share = jnp.exp(past_peak - peak)
    new_weight = jnp.exp(new_scores - peak[:, :, None])
    denominator = past_total * past_share + jnp.sum(new_weight, axis=-1)
    latent_sum = (past_sum * past_share[..., None]).astype(jnp.bfloat16)
    head_values = value_up_weight.reshape(latent_width, heads_local, VALUE_WIDTH)
    past_out = jnp.einsum(
        "shk,khd->shd", latent_sum, head_values, preferred_element_type=jnp.float32
    )
    new_out = jnp.einsum(
        "shp,sphd->shd",
        new_weight.astype(jnp.bfloat16),
        new_values.reshape(owned, fresh, heads_local, VALUE_WIDTH),
        preferred_element_type=jnp.float32,
    )
    attended = (
        ((past_out + new_out) / denominator[:, :, None])
        .astype(jnp.bfloat16)
        .reshape(owned, heads_local * VALUE_WIDTH)
    )
    return (new_keys, new_values, new_rope, attended)


def solution(mesh):
    in_specs = (
        P(None, "sp", "tp"),
        P(),
        P(),
        P(),
        P(None, "tp"),
        P(None, "tp"),
        P("sp", "tp", None),
        P("sp", "tp", None),
        P("sp", "tp"),
        P("sp", "tp"),
    )
    out_specs = (P("sp", None, "tp"), P("sp", None, "tp"), P("sp", None, None), P("sp", "tp"))
    return jax.shard_map(
        on_device, mesh=mesh, in_specs=in_specs, out_specs=out_specs, check_vma=False
    )
```

profile of v0, /device:TPU:0, one launch (start us, length us, event | category | flops | bytes accessed | tf_op | source)
XLA Modules:
  0.0 66.8 jit_solution(9695988542635753334)
XLA Ops:
  0.6 1.8 %copy.21 = bf16[8,10,1024]{2,1,0:T(8,128)(2,1)} copy(bf16[8,10,1024]{2,0,1:T(8,128)(2,1)} %param.12) | data formatting | bytes 327680 | tf_op args[0]
  2.4 7.3 %all-to-all-start = ((bf16[8,10,1024]{2,1,0:T(8,128)(2,1)}), bf16[8,10,1024]{2,1,0:T(8,128)(2,1)}, u32[]{:S(2)}, u32[]{:S(2)}) async-start(bf16[8,10,1024]{2,1,0:T(8,128)(2,1)} %copy.21), calls=%async_computation | async-start | bytes 524288 | tf_op jit(solution)/shard_map/all_to_all | solution.py:63
  9.7 0.7 %reduce.8 = bf16[512]{0:T(512)(128)(2,1)S(1)} reduce(bf16[1,512]{1,0:T(2,128)(2,1)} %param.21, bf16[]{:T(256)} %constant.97), dimensions={0}, to_apply=%param.21.reduce_sub_computation | reduce | bytes 2050 | tf_op args[9]
  10.4 0.1 reshape.326
  10.5 5.2 %all_gather.29 = bf16[1,32,64]{2,1,0:T(8,128)(2,1)S(1)} all-gather(bf16[1,8,64]{2,1,0:T(8,128)(2,1)S(1)} %reshape.326), channel_id=1, replica_groups=mesh['sp'=8,'tp'=4] {'tp'}, dimensions={1}, use_global_device_ids=true | all-gather | bytes 5120 | tf_op jit(solution)/shard_map/all_gather | solution.py:101
  15.7 1.6 %fusion.18 = bf16[8,1,512]{2,1,0:T(2,128)(2,1)S(1)} fusion(bf16[1,1024]{1,0:T(2,128)(2,1)} %param.20, bf16[512,1024]{1,0:T(8,128)(2,1)} %param.16), kind=kOutput, calls=%fused_computation.28 | convolution fusion | flops 1048576 | bytes 1058816 | tf_op jit(solution)/shard_map/shd,khd->shk/dot_general | solution.py:96
  17.3 5.2 %all-gather = bf16[32,512]{1,0:T(8,128)(2,1)S(1)} all-gather(bf16[8,512]{1,0:T(8,128)(2,1)S(1)} %bitcast.161), channel_id=2, replica_groups=mesh['sp'=8,'tp'=4] {'tp'}, dimensions={0}, use_global_device_ids=true | all-gather | bytes 40960 | tf_op jit(solution)/shard_map/all_gather | solution.py:100
  22.5 5.9 %fusion.11 = f32[32,8192]{1,0:T(8,128)S(1)} fusion(bf16[32,512]{1,0:T(8,128)(2,1)S(1)} %all-gather, bf16[1,8192,512]{2,1,0:T(8,128)(2,1)} %param.18), kind=kOutput, calls=%fused_computation.17 | convolution fusion | flops 268435456 | bytes 9469952 | tf_op jit(solution)/shard_map/shk,spk->shp/dot_general | solution.py:103
  28.4 0.4 fusion.64
  28.8 0.4 fusion.23
  29.2 0.6 dynamic-slice
  30.5 0.2 dynamic-update-slice
  30.7 0.2 dynamic-update-slice.1
  30.9 7.1 %all-reduce.2 = (f32[128]{0:T(128)S(1)}, f32[128]{0:T(128)S(1)}) all-reduce(f32[128]{0:T(128)S(1)} %dynamic-update-slice, f32[128]{0:T(128)S(1)} %dynamic-update-slice.1), channel_id=3, replica_groups=mesh['sp'=8,'tp'=4] {'tp'}, use_global_device_ids=true, to_apply=%add | all-reduce | flops 256 | bytes 2048
  38.0 0.1 reshape.336
  38.2 5.1 %fusion.9 = f32[32,512]{1,0:T(8,128)S(1)} fusion(bf16[1,8192,512]{2,1,0:T(8,128)(2,1)} %param.18, f32[32,8192]{1,0:T(8,128)S(1)} %get-tuple-element.237, f32[32]{0:T(128)S(1)} %get-tuple-element.236), kind=kOutput, calls=%fused_computation.15 | convolution fusion | flops 268959744 | bytes 9502848 | tf_op jit(solution)/shard_map/shp,spk->shk/dot_general | solution.py:113
  43.2 5.9 %all-gather.3 = f32[128,512]{1,0:T(8,128)S(1)} all-gather(f32[32,512]{1,0:T(8,128)S(1)} %fusion.9), channel_id=5, replica_groups=mesh['sp'=8,'tp'=4] {'tp'}, dimensions={0}, use_global_device_ids=true | all-gather | bytes 327680 | tf_op jit(solution)/shard_map/all_gather | solution.py:17
  49.2 0.5 while.19
  49.7 1.0 %all_to_all.10 = bf16[1,80,1024]{2,1,0:T(8,128)(2,1)S(1)} reshape(bf16[8,10,1024]{2,1,0:T(8,128)(2,1)} %all-to-all-done) | data formatting | bytes 327680 | tf_op jit(solution)/shard_map/all_to_all | solution.py:63
  50.7 8.0 %all_gather.27 = bf16[1,80,4096]{2,1,0:T(8,128)(2,1)S(1)} all-gather(bf16[1,80,1024]{2,1,0:T(8,128)(2,1)S(1)} %all_to_all.10), channel_id=1, replica_groups=mesh['sp'=8,'tp'=4] {'tp'}, dimensions={2}, use_global_device_ids=true | all-gather | bytes 819200 | tf_op jit(solution)/shard_map/all_gather | solution.py:69
  58.7 3.1 %multiply_reduce_fusion = (f32[80]{0:T(128)S(1)}, f32[80,512]{1,0:T(8,128)S(1)}) fusion(bf16[4096,512]{1,0:T(8,128)(2,1)} %param.13, bf16[1,80,4096]{2,1,0:T(8,128)(2,1)S(1)} %all_gather.27), kind=kOutput, calls=%fused_computation.46 | convolution fusion | flops 335626176 | bytes 5013824 | tf_op jit(solution)/shard_map/dot_general | solution.py:72
  61.9 0.4 convolution_convert_fusion.1
  62.3 0.2 fusion.32
  62.5 1.4 %convolution_bitcast_fusion = f32[1,80,64]{1,2,0:T(8,128)S(1)} fusion(bf16[4096,64]{0,1:T(8,128)(2,1)} %param.14, bf16[1,80,4096]{2,1,0:T(8,128)(2,1)S(1)} %all_gather.27), kind=kOutput, calls=%fused_computation.21 | convolution fusion | flops 41943040 | bytes 1200128 | tf_op jit(solution)/shard_map/dot_general | solution.py:73
  63.9 0.4 convolution_convert_fusion
  64.3 0.1 fusion.40
  64.4 0.6 pad_maximum_fusion
  65.0 0.2 fusion.63
  65.3 0.2 fusion.54
  65.7 0.3 fusion.15
  66.0 0.2 fusion.29
  66.2 0.6 copy.64
  (43 shorter events, 0.9 us)
Async XLA Ops:
  0.6 27.8 %copy-start = (bf16[1,8192,64]{1,2,0:T(8,128)(2,1)S(1)}, bf16[1,8192,64]{1,2,0:T(8,128)(2,1)}, u32[]{:S(2)}) copy-start(bf16[1,8192,64]{1,2,0:T(8,128)(2,1)} %param.19) | copy-start | bytes 3145732
  2.4 47.3 %all-to-all-start = ((bf16[8,10,1024]{2,1,0:T(8,128)(2,1)}), bf16[8,10,1024]{2,1,0:T(8,128)(2,1)}, u32[]{:S(2)}, u32[]{:S(2)}) async-start(bf16[8,10,1024]{2,1,0:T(8,128)(2,1)} %copy.21), calls=%async_computation | async-start | bytes 524288 | tf_op jit(solution)/shard_map/all_to_all | solution.py:63
  22.5 6.7 %copy-start.7 = (u32[32]{0:T(128)S(1)}, u32[32]{0:T(128)}, u32[]{:S(2)}) copy-start(u32[32]{0:T(128)} %constant.87) | copy-start | bytes 388
  38.2 23.7 %copy-start.1 = (bf16[512,1024]{1,0:T(8,128)(2,1)S(1)}, bf16[512,1024]{1,0:T(8,128)(2,1)}, u32[]{:S(2)}) copy-start(bf16[512,1024]{1,0:T(8,128)(2,1)} %param.16) | copy-start | bytes 3145732
  38.2 23.7 %copy-start.5 = (f32[512]{0:T(512)S(1)}, f32[512]{0:T(512)}, u32[]{:S(2)}) copy-start(f32[512]{0:T(512)} %param.15) | copy-start | bytes 6148
  43.2 19.0 %copy-start.6 = (bf16[1,1024]{1,0:T(2,128)(2,1)S(1)}, bf16[1,1024]{1,0:T(2,128)(2,1)}, u32[]{:S(2)}) copy-start(bf16[1,1024]{1,0:T(2,128)(2,1)} %param.20) | copy-start | bytes 6148
  43.2 20.7 %copy-start.2 = (bf16[512,1024]{1,0:T(8,128)(2,1)S(1)}, bf16[512,1024]{1,0:T(8,128)(2,1)}, u32[]{:S(2)}) copy-start(bf16[512,1024]{1,0:T(8,128)(2,1)} %param.17) | copy-start | bytes 3145732
  62.3 4.5 %copy-start.3 = (bf16[80,1024]{1,0:T(8,128)(2,1)}, bf16[80,1024]{1,0:T(8,128)(2,1)S(1)}, u32[]{:S(2)}) copy-start(bf16[80,1024]{1,0:T(8,128)(2,1)S(1)} %convolution_convert_fusion.1) | copy-start | bytes 491524
  64.3 2.6 %copy-start.4 = (bf16[80,1024]{1,0:T(8,128)(2,1)}, bf16[80,1024]{1,0:T(8,128)(2,1)S(1)}, u32[]{:S(2)}) copy-start(bf16[80,1024]{1,0:T(8,128)(2,1)S(1)} %convolution_convert_fusion) | copy-start | bytes 491524
where the time goes:
time: 67.3 us; the launch traced here: 66.8 us
  blocking collectives  31.4 us (47%)
  matrix products  19.1 us (28%)
  starting transfers between devices  7.28 us (11%)
  local copies, waits for them, and re-layouts  4.87 us (7%)
  other arithmetic  2.69 us (4%)
  between operations  1.45 us (2%)
    all_gather x1, blocking collectives, on_device(): fragment = lax.all_gather(rows_here, 'tp', axis=2, tiled=True)  7.99 us
    all_to_all x1, starting transfers between devices, on_device(): lax.all_to_all(tokens, 'sp', split_axis=0, concat_axis=1, tiled=True)  7.28 us
    unnamed x1, blocking collectives  7.09 us
    dot_general x1, matrix products, on_device(): jnp.einsum('shk,spk->shp', every_latent, cached_latent_rows, preferred_el...  5.92 us
    all_gather x1, blocking collectives, combined_all(): gathered = jax.tree.map(lambda a: lax.all_gather(a, axis), part)  5.91 us
    all_gather x1, blocking collectives, on_device(): lax.all_gather(query_latent, 'tp', axis=1, tiled=True)  5.19 us
    all_gather x1, blocking collectives, on_device(): lax.all_gather(turn_own, 'tp', axis=1, tiled=True)  5.18 us
    dot_general x1, matrix products, on_device(): jnp.einsum('shp,spk->shk', local_weight.astype(jnp.bfloat16), cached_late...  5.06 us
  transfers between devices with their start and end apart: 1, of which 0 were waited for; matrix products, arithmetic and copies ran while one was open for 24% of the time, Pallas kernels for 0%

commit v1 on v0

v1 whole, which is shorter than its diff:
```python
import functools

import jax
import jax.numpy as jnp
import numpy as np
from jax import lax
from jax.experimental import pallas as pl
from jax.experimental.pallas import tpu as pltpu
from jax.sharding import PartitionSpec as P

PLAIN_KEY_WIDTH = 128
ROPE = 64
VALUE_WIDTH = 128
PAST_POSITIONS = 32768

epsilon = 1e-06
rope_theta = 10000.0
MESH = pl.DeviceIdType.MESH
F32 = jnp.float32
BF16 = jnp.bfloat16
LANES = 128


def up_to(n, m):
    return -(-n // m) * m


def dot(a, b, ca, cb):
    return lax.dot_general(a, b, (((ca,), (cb,)), ((), ())), preferred_element_type=F32)


def head_mask(shape, width):
    row = lax.broadcasted_iota(jnp.int32, shape, 0) * width
    col = lax.broadcasted_iota(jnp.int32, shape, 1)
    return (col >= row) & (col < row + width)


def kernel(cfg, *refs):
    (tok_h, wd_h, wr_h, gain_h, ku_h, vu_h, cache_h, prope_h, qn_h, qr_h,
     perm_h, sel_h, fold_h, table_h,
     keys_h, vals_h, rope_h, att_h,
     tok, wd, wr, gain, ku, vu, cache, prope, qn, qr, perm, sel, fold, table,
     keys_v, vals_v, rope_v, att_v,
     q_send, q_recv, part_send, part_recv, lat_send, lat_recv, a_send, a_recv, scores,
     load_sem, cache_sem, out_sem,
     q_ss, q_rs, p_ss, p_rs, l_ss, l_rs, a_ss, a_rs) = refs
    nsp, ntp, groups, npos, heads, chunk, chunks = (
        cfg[k] for k in ("nsp", "ntp", "groups", "npos", "heads", "chunk", "chunks"))
    feat, lw, gp, slot = cfg["feat"], cfg["lw"], cfg["gp"], cfg["slot"]
    s = lax.axis_index("sp")
    t = lax.axis_index("tp")
    factor = (PLAIN_KEY_WIDTH + ROPE) ** (-0.5)

    copies = {}

    def load(name, src, dst):
        c = pltpu.make_async_copy(src, dst, load_sem.at[len(copies)])
        c.start()
        copies[name] = c

    rows0 = pl.multiple_of(t * feat, LANES)
    load("qn", qn_h, qn)
    load("qr", qr_h, qr)
    load("ku", ku_h, ku)
    load("fold", fold_h, fold)
    load("tok", tok_h, tok)
    load("perm", perm_h, perm)
    load("wd", wd_h.at[pl.ds(rows0, feat), :], wd)
    load("wr", wr_h.at[:, pl.ds(rows0, feat)], wr)
    load("gain", gain_h, gain)
    load("table", table_h.at[s], table)
    load("sel", sel_h, sel)
    load("prope", prope_h, prope)
    cache_copies = []
    for c in range(chunks):
        cc = pltpu.make_async_copy(
            cache_h.at[pl.ds(c * chunk, chunk), :], cache.at[pl.ds(c * chunk, chunk), :], cache_sem.at[c])
        cc.start()
        cache_copies.append(cc)
    load("vu", vu_h, vu)

    barrier = pltpu.get_barrier_semaphore()
    for d in range(1, ntp):
        pl.semaphore_signal(barrier, inc=1, device_id=(s, lax.rem(t + d, ntp)), device_id_type=MESH)
    from_t = lax.rem(s, ntp)
    for src in range(nsp):
        @pl.when(src != s)
        def _():
            pl.semaphore_signal(barrier, inc=1, device_id=(src, from_t), device_id_type=MESH)

    for name in ("qn", "qr", "ku", "fold"):
        copies[name].wait()
    qn_row = jnp.broadcast_to(qn[...].astype(F32), (heads, qn.shape[1]))
    q_bd = jnp.where(head_mask(qn_row.shape, PLAIN_KEY_WIDTH), qn_row, 0.0).astype(BF16)
    qr_row = jnp.broadcast_to(qr[...].astype(F32), (heads, qr.shape[1]))
    qr_bd = jnp.where(head_mask(qr_row.shape, ROPE), qr_row, 0.0).astype(BF16)
    q_lat = dot(q_bd, ku[...], 1, 1).astype(BF16).astype(F32)
    q_rot = dot(qr_bd, fold[...], 1, 0)
    q_own = jnp.concatenate([q_lat, q_rot], axis=1)
    q_send[...] = q_own
    q_recv[t] = q_own

    self_row = from_t == t
    pl.semaphore_wait(
        barrier, ntp - 1 + ntp * groups - ntp * jnp.where(self_row, 1, 0).astype(jnp.int32))

    def peer_copy(src, dst, ssem, rsem, peer):
        return pltpu.make_async_remote_copy(
            src_ref=src, dst_ref=dst, send_sem=ssem, recv_sem=rsem,
            device_id=(s, peer), device_id_type=MESH)

    pending = []
    for d in range(1, ntp):
        c = peer_copy(q_send, q_recv.at[t], q_ss.at[d], q_rs.at[t], lax.rem(t + d, ntp))
        c.start()
        pending.append(c)

    for name in ("tok", "perm", "wd", "wr"):
        copies[name].wait()
    rows = dot(perm[...], tok[...], 1, 0).astype(BF16)
    lat_part = dot(rows, wd[...], 1, 0)
    rope_part = dot(rows, wr[...], 1, 1)
    for u in range(ntp):
        part_send[u, :, :lw] = lat_part[u * gp:(u + 1) * gp]
        part_send[u, :, lw:lw + ROPE] = rope_part[u * gp:(u + 1) * gp]
        part_send[u, :, lw + ROPE:] = jnp.zeros((gp, LANES - ROPE), F32)
    for d in range(1, ntp):
        peer = lax.rem(t + d, ntp)
        c = peer_copy(part_send.at[peer], part_recv.at[t], p_ss.at[d], p_rs.at[t], peer)
        c.start()
        pending.append(c)

    for d in range(1, ntp):
        peer = lax.rem(t + d, ntp)
        peer_copy(q_recv.at[peer], q_recv.at[peer], q_ss.at[d], q_rs.at[peer], peer).wait_recv()
    q_all = jnp.concatenate([q_recv[u] for u in range(ntp)], axis=0)
    q_all_lat = q_all[:, :lw].astype(BF16)
    q_all_rot = q_all[:, lw:lw + ROPE].astype(BF16)
    copies["prope"].wait()
    high = None
    for c in range(chunks):
        cache_copies[c].wait()
        cols = slice(c * chunk, (c + 1) * chunk)
        sc = (dot(q_all_lat, cache[cols, :], 1, 1) + dot(q_all_rot, prope[:, cols], 1, 0)) * factor
        scores[:, cols] = sc
        top = jnp.max(sc, axis=1, keepdims=True)
        high = top if high is None else jnp.maximum(high, top)

    total = part_send[t]
    for d in range(1, ntp):
        peer = lax.rem(t + d, ntp)
        peer_copy(part_recv.at[peer], part_recv.at[peer], p_ss.at[d], p_rs.at[peer], peer).wait_recv()
        total = total + part_recv[peer]
    copies["gain"].wait()
    copies["table"].wait()
    raw = total[:, :lw]
    scale = lax.rsqrt(jnp.mean(raw * raw, axis=-1, keepdims=True) + epsilon)
    latent = raw * scale * gain[...]
    turn = total[:, lw:lw + ROPE]
    half = ROPE // 2
    swapped = jnp.concatenate([turn[:, half:], turn[:, :half]], axis=1)
    turned = turn * table[:, :ROPE] + swapped * table[:, ROPE:]
    both = jnp.concatenate([latent, turned, jnp.zeros((gp, LANES - ROPE), F32)], axis=1)
    for k in range(groups):
        block = both[k * npos:(k + 1) * npos]
        if slot > npos:
            block = jnp.concatenate([block, jnp.zeros((slot - npos, both.shape[1]), F32)], axis=0)
        lat_send[k] = block.astype(BF16)

    def row_copy(k, d):
        return pltpu.make_async_remote_copy(
            src_ref=lat_send.at[k], dst_ref=lat_recv.at[s],
            send_sem=l_ss.at[k * ntp + d], recv_sem=l_rs.at[s],
            device_id=(k * ntp + t, lax.rem(t + d, ntp)), device_id_type=MESH)

    for k in range(groups):
        for d in range(1, ntp):
            c = row_copy(k, d)
            c.start()
            pending.append(c)

        @pl.when(k * ntp + t != s)
        def _():
            row_copy(k, 0).start()

        @pl.when(k * ntp + t == s)
        def _():
            lat_recv[s] = lat_send[k]

    summed = None
    mass = None
    for c in range(chunks):
        cols = slice(c * chunk, (c + 1) * chunk)
        w = jnp.exp(scores[:, cols] - high)
        part = jnp.sum(w, axis=1, keepdims=True)
        mass = part if mass is None else mass + part
        o = dot(w.astype(BF16), cache[cols, :], 1, 0)
        summed = o if summed is None else summed + o
    stats_lane = lax.broadcasted_iota(jnp.int32, (summed.shape[0], LANES), 1)
    stats = jnp.where(stats_lane < LANES // 2, high, mass)
    partial = jnp.concatenate([summed, stats], axis=1)
    for u in range(ntp):
        a_send[u] = partial[u * heads:(u + 1) * heads]
    for d in range(1, ntp):
        peer = lax.rem(t + d, ntp)
        c = peer_copy(a_send.at[peer], a_recv.at[t], a_ss.at[d], a_rs.at[t], peer)
        c.start()
        pending.append(c)

    for src in range(nsp):
        def arrive(src=src):
            pltpu.make_async_remote_copy(
                src_ref=lat_send.at[0], dst_ref=lat_recv.at[src],
                send_sem=l_ss.at[0], recv_sem=l_rs.at[src],
                device_id=(src, from_t), device_id_type=MESH).wait_recv()

        pl.when(jnp.logical_or(src != s, jnp.logical_not(self_row)))(arrive)
    copies["sel"].wait()
    copies["vu"].wait()
    arrived = lat_recv[...].reshape(nsp * slot, lw + LANES)
    block_lat = dot(sel[...], arrived[:, :lw], 1, 0).astype(BF16)
    new_turn = dot(arrived[:, lw:], sel[...], 0, 1)[:ROPE].astype(BF16)
    new_k = dot(block_lat, ku[...], 1, 0).astype(BF16)
    new_v = dot(block_lat, vu[...], 1, 0).astype(BF16)
    keys_v[...] = new_k
    vals_v[...] = new_v
    rope_v[...] = new_turn
    outs = [(keys_v, keys_h), (vals_v, vals_h), (rope_v, rope_h)]
    for i, (a, b) in enumerate(outs):
        pltpu.make_async_copy(a, b, out_sem.at[i]).start()

    new_scores = (dot(q_bd, new_k, 1, 1) + dot(q_rot[:, :ROPE].astype(BF16), new_turn, 1, 0)) * factor
    peak = jnp.max(new_scores, axis=1, keepdims=True)
    own = a_send[t]
    for d in range(1, ntp):
        peer = lax.rem(t + d, ntp)
        peer_copy(a_recv.at[peer], a_recv.at[peer], a_ss.at[d], a_rs.at[peer], peer).wait_recv()
    parts = [own] + [a_recv[lax.rem(t + d, ntp)] for d in range(1, ntp)]
    for p in parts:
        peak = jnp.maximum(peak, p[:, lw:lw + 1])
    new_w = jnp.exp(new_scores - peak)
    denom = jnp.sum(new_w, axis=1, keepdims=True)
    past = None
    for p in parts:
        share = jnp.exp(p[:, lw:lw + 1] - peak)
        denom = denom + p[:, lw + LANES // 2:lw + LANES // 2 + 1] * share
        o = p[:, :lw] * share
        past = o if past is None else past + o
    out = dot(past.astype(BF16), vu[...], 1, 0) + dot(new_w.astype(BF16), new_v, 1, 0)
    out = out / denom
    att_v[...] = jnp.sum(
        jnp.where(head_mask(out.shape, VALUE_WIDTH), out, 0.0), axis=0, keepdims=True).astype(BF16)
    last = pltpu.make_async_copy(att_v, att_h, out_sem.at[len(outs)])
    last.start()

    for c in pending:
        c.wait_send()
    for k in range(groups):
        @pl.when(k * ntp + t != s)
        def _():
            row_copy(k, 0).wait_send()
    for i, (a, b) in enumerate(outs):
        pltpu.make_async_copy(a, b, out_sem.at[i]).wait()
    last.wait()


def solution(mesh):
    nsp, ntp = mesh.shape["sp"], mesh.shape["tp"]

    def on_device(tokens, wd, wr, gain, ku, vu, cached, prope, qn, qr):
        prompts, npos, feat = tokens.shape
        owned, past, lw = cached.shape
        assert owned == 1 and prompts == nsp and prompts % ntp == 0
        turn = wr.shape[1]
        hk, hv = ku.shape[1], vu.shape[1]
        heads = qn.shape[1] // PLAIN_KEY_WIDTH
        groups = prompts // ntp
        gp = up_to(groups * npos, 8)
        slot = up_to(npos, 16)
        fresh = nsp * npos
        chunk = min(past, 1024)
        chunks = past // chunk
        width = lw + LANES

        perm = np.zeros((ntp * gp, prompts * npos), np.float32)
        table = np.zeros((nsp, gp, 2 * turn), np.float32)
        half = turn // 2
        freq = rope_theta ** (-np.arange(half) / half)
        for k in range(groups):
            for j in range(npos):
                i = k * npos + j
                for u in range(ntp):
                    perm[u * gp + i, j * prompts + k * ntp + u] = 1
                for sp in range(nsp):
                    a = (PAST_POSITIONS + sp * npos + j) * freq
                    table[sp, i] = np.concatenate([np.cos(a), np.cos(a), -np.sin(a), np.sin(a)])
        sel = np.zeros((fresh, nsp * slot), np.float32)
        for sp in range(nsp):
            for j in range(npos):
                sel[sp * npos + j, sp * slot + j] = 1
        fold = np.zeros((heads * turn, LANES), np.float32)
        fold[np.arange(heads * turn), np.arange(heads * turn) % turn] = 1

        cfg = dict(nsp=nsp, ntp=ntp, groups=groups, npos=npos, heads=heads, chunk=chunk,
                   chunks=chunks, feat=feat, lw=lw, gp=gp, slot=slot)
        args = (
            tokens.transpose(1, 0, 2).reshape(npos * prompts, feat),
            wd, wr.T, gain.reshape(1, lw), ku, vu,
            cached.reshape(past, lw), prope.reshape(past, turn).T, qn, qr,
            jnp.asarray(perm, BF16), jnp.asarray(sel, BF16), jnp.asarray(fold, BF16),
            jnp.asarray(table),
        )
        v = pltpu.VMEM
        dma = pltpu.SemaphoreType.DMA
        scratch = [
            v(args[0].shape, BF16), v((feat, lw), BF16), v((turn, feat), BF16), v((1, lw), F32),
            v(ku.shape, BF16), v(vu.shape, BF16), v((past, lw), BF16), v((turn, past), BF16),
            v(qn.shape, BF16), v(qr.shape, BF16),
            v(perm.shape, BF16), v(sel.shape, BF16), v(fold.shape, BF16), v(table.shape[1:], F32),
            v((fresh, hk), BF16), v((fresh, hv), BF16), v((turn, fresh), BF16), v((1, hv), BF16),
            v((heads, width), F32), v((ntp, heads, width), F32),
            v((ntp, gp, width), F32), v((ntp, gp, width), F32),
            v((groups, slot, width), BF16), v((nsp, slot, width), BF16),
            v((ntp, heads, width), F32), v((ntp, heads, width), F32),
            v((ntp * heads, past), F32),
            dma((13,)), dma((chunks,)), dma((4,)),
            dma((ntp,)), dma((ntp,)), dma((ntp,)), dma((ntp,)),
            dma((groups * ntp,)), dma((nsp,)), dma((ntp,)), dma((ntp,)),
        ]
        any_spec = pl.BlockSpec(memory_space=pl.ANY)
        keys, vals, rope, att = pl.pallas_call(
            functools.partial(kernel, cfg),
            out_shape=(
                jax.ShapeDtypeStruct((fresh, hk), BF16),
                jax.ShapeDtypeStruct((fresh, hv), BF16),
                jax.ShapeDtypeStruct((turn, fresh), BF16),
                jax.ShapeDtypeStruct((1, hv), BF16),
            ),
            in_specs=[any_spec] * len(args),
            out_specs=(any_spec,) * 4,
            scratch_shapes=scratch,
            compiler_params=pltpu.CompilerParams(
                collective_id=0, has_side_effects=True, vmem_limit_bytes=60 * 1024 * 1024),
        )(*args)
        return (
            keys.reshape(1, fresh, hk),
            vals.reshape(1, fresh, hv),
            rope.T.reshape(1, fresh, turn),
            att,
        )

    in_specs = (
        P(None, "sp", "tp"),
        P(),
        P(),
        P(),
        P(None, "tp"),
        P(None, "tp"),
        P("sp", "tp", None),
        P("sp", "tp", None),
        P("sp", "tp"),
        P("sp", "tp"),
    )
    out_specs = (P("sp", None, "tp"), P("sp", None, "tp"), P("sp", None, None), P("sp", "tp"))
    return jax.shard_map(
        on_device, mesh=mesh, in_specs=in_specs, out_specs=out_specs, check_vma=False
    )
```

time: 67.3 us -> 32.4 us (0.48)
  blocking collectives: 31.4 us -> 0 us
  Pallas kernels: 0 us -> 25.7 us
  matrix products: 19.1 us -> 0 us
  starting transfers between devices: 7.28 us -> 0 us
  other arithmetic: 2.69 us -> 0 us
  local copies, waits for them, and re-layouts: 4.87 us -> 5.78 us
  between operations: 1.45 us -> 0.64 us
    pallas_call x0 -> x1, Pallas kernels: none -> 25.7 us  [on_device(): pl.pallas_call(functools.partial(kernel, cfg), out_shape=(jax.ShapeDtypeS...]
    all_gather x4 -> x0, blocking collectives: 24.3 us -> none  [the longest x1 7.99 us: on_device(): fragment = lax.all_gather(rows_here, 'tp', axis=2, tiled=True)]
    dot_general x12 -> x0, matrix products: 19.1 us -> none  [the longest x1 5.92 us: on_device(): jnp.einsum('shk,spk->shp', every_latent, cached_latent_rows, preferred_el...]
    all_to_all x1 -> x0, starting transfers between devices: 7.28 us -> none  [on_device(): lax.all_to_all(tokens, 'sp', split_axis=0, concat_axis=1, tiled=True)]
    unnamed x1 -> x0, blocking collectives: 7.09 us -> none
    unnamed x23 -> x4, local copies, waits for them, and re-layouts: 3.5 us -> 5.78 us
    all_to_all x1 -> x0, local copies, waits for them, and re-layouts: 1.01 us -> none  [on_device(): lax.all_to_all(tokens, 'sp', split_axis=0, concat_axis=1, tiled=True)]
    unnamed x2 -> x0, other arithmetic: 0.77 us -> none
  transfers between devices with their start and end apart: 1 -> 0, of which waited for: 0 -> 0; matrix products, arithmetic and copies ran while one was open for 24% -> 0% of each run, Pallas kernels for 0% -> 0%
where the time goes in v1:
time: 32.4 us; the launch traced here: 32.1 us
  Pallas kernels  25.7 us (79%)
  local copies, waits for them, and re-layouts  5.78 us (18%)
  between operations  0.64 us (2%)
    pallas_call x1, Pallas kernels, on_device(): pl.pallas_call(functools.partial(kernel, cfg), out_shape=(jax.ShapeDtypeS...  25.7 us
    unnamed x4, local copies, waits for them, and re-layouts  5.78 us

profile of v1, /device:TPU:0, one launch (start us, length us, event | category | flops | bytes accessed | tf_op | source)
XLA Modules:
  0.0 32.1 jit_solution(15964016954799855268)
XLA Ops:
  0.6 25.7 %shard_map.165 = (bf16[80,1024]{1,0:T(8,128)(2,1)}, bf16[80,1024]{1,0:T(8,128)(2,1)}, bf16[64,80]{1,0:T(8,128)(2,1)}, bf16[1,1024]{1,0:T(2,128)(2,1)}) custom-call(bf16[80,1024]{1,0:T(8,128)(2,1)} %bitcast.17, bf16[4096,512]{1,0:T(8,128)(2,1)} %refs_1_.1, bf16[64,4096]{1,0:T(8,128)(2,1)} %bitcast.16, f32[1,512]{1,0:T(1,128)} %bitcast.21, ...), custom_call_target="tpu_custom_call" | custom-call | tf_op jit(solution)/shard_map/pallas_call | solution.py:331
  26.3 1.6 %copy.22 = bf16[1,80,1024]{2,1,0:T(8,128)(2,1)} copy(bf16[1,80,1024]{2,1,0:T(8,128)(2,1)} %bitcast.19) | data formatting | bytes 327680
  27.9 1.6 %copy.23 = bf16[1,80,1024]{2,1,0:T(8,128)(2,1)} copy(bf16[1,80,1024]{2,1,0:T(8,128)(2,1)} %bitcast.18) | data formatting | bytes 327680
  29.5 1.3 %copy.24 = bf16[1,80,64]{1,2,0:T(8,128)(2,1)} copy(bf16[1,80,64]{1,2,0:T(8,128)(2,1)} %bitcast.20) | data formatting | bytes 20480
  30.8 1.3 %copy.25 = bf16[1,1024]{1,0:T(2,128)(2,1)} copy(bf16[1,1024]{1,0:T(2,128)(2,1)} %get-tuple-element.19) | data formatting | bytes 4096

commit v2 on v1

--- a/solution.py
+++ b/solution.py
@@ -38,11 +38,10 @@
 def kernel(cfg, *refs):
     (tok_h, wd_h, wr_h, gain_h, ku_h, vu_h, cache_h, prope_h, qn_h, qr_h,
      perm_h, sel_h, fold_h, table_h,
-     keys_h, vals_h, rope_h, att_h,
+     keys_v, vals_v, rope_v, att_v,
      tok, wd, wr, gain, ku, vu, cache, prope, qn, qr, perm, sel, fold, table,
-     keys_v, vals_v, rope_v, att_v,
      q_send, q_recv, part_send, part_recv, lat_send, lat_recv, a_send, a_recv, scores,
-     load_sem, cache_sem, out_sem,
+     load_sem, cache_sem,
      q_ss, q_rs, p_ss, p_rs, l_ss, l_rs, a_ss, a_rs) = refs
     nsp, ntp, groups, npos, heads, chunk, chunks = (
         cfg[k] for k in ("nsp", "ntp", "groups", "npos", "heads", "chunk", "chunks"))
@@ -225,9 +224,6 @@
     keys_v[...] = new_k
     vals_v[...] = new_v
     rope_v[...] = new_turn
-    outs = [(keys_v, keys_h), (vals_v, vals_h), (rope_v, rope_h)]
-    for i, (a, b) in enumerate(outs):
-        pltpu.make_async_copy(a, b, out_sem.at[i]).start()
 
     new_scores = (dot(q_bd, new_k, 1, 1) + dot(q_rot[:, :ROPE].astype(BF16), new_turn, 1, 0)) * factor
     peak = jnp.max(new_scores, axis=1, keepdims=True)
@@ -250,8 +246,6 @@
     out = out / denom
     att_v[...] = jnp.sum(
         jnp.where(head_mask(out.shape, VALUE_WIDTH), out, 0.0), axis=0, keepdims=True).astype(BF16)
-    last = pltpu.make_async_copy(att_v, att_h, out_sem.at[len(outs)])
-    last.start()
 
     for c in pending:
         c.wait_send()
@@ -259,9 +253,16 @@
         @pl.when(k * ntp + t != s)
         def _():
             row_copy(k, 0).wait_send()
-    for i, (a, b) in enumerate(outs):
-        pltpu.make_async_copy(a, b, out_sem.at[i]).wait()
-    last.wait()
+
+
+def put_out(*refs):
+    sem = refs[-1]
+    count = (len(refs) - 1) // 2
+    copies = [pltpu.make_async_copy(refs[i], refs[count + i], sem.at[i]) for i in range(count)]
+    for c in copies:
+        c.start()
+    for c in copies:
+        c.wait()
 
 
 def solution(mesh):
@@ -317,31 +318,35 @@
             v(ku.shape, BF16), v(vu.shape, BF16), v((past, lw), BF16), v((turn, past), BF16),
             v(qn.shape, BF16), v(qr.shape, BF16),
             v(perm.shape, BF16), v(sel.shape, BF16), v(fold.shape, BF16), v(table.shape[1:], F32),
-            v((fresh, hk), BF16), v((fresh, hv), BF16), v((turn, fresh), BF16), v((1, hv), BF16),
             v((heads, width), F32), v((ntp, heads, width), F32),
             v((ntp, gp, width), F32), v((ntp, gp, width), F32),
             v((groups, slot, width), BF16), v((nsp, slot, width), BF16),
             v((ntp, heads, width), F32), v((ntp, heads, width), F32),
             v((ntp * heads, past), F32),
-            dma((13,)), dma((chunks,)), dma((4,)),
+            dma((13,)), dma((chunks,)),
             dma((ntp,)), dma((ntp,)), dma((ntp,)), dma((ntp,)),
             dma((groups * ntp,)), dma((nsp,)), dma((ntp,)), dma((ntp,)),
         ]
         any_spec = pl.BlockSpec(memory_space=pl.ANY)
-        keys, vals, rope, att = pl.pallas_call(
+        shapes = ((fresh, hk), (fresh, hv), (turn, fresh), (1, hv))
+        room = 66_900_000 - sum(2 * up_to(r, 16) * up_to(c, LANES) for r, c in shapes)
+        made = pl.pallas_call(
             functools.partial(kernel, cfg),
-            out_shape=(
-                jax.ShapeDtypeStruct((fresh, hk), BF16),
-                jax.ShapeDtypeStruct((fresh, hv), BF16),
-                jax.ShapeDtypeStruct((turn, fresh), BF16),
-                jax.ShapeDtypeStruct((1, hv), BF16),
-            ),
+            out_shape=tuple(pltpu.VMEM(shape, BF16) for shape in shapes),
             in_specs=[any_spec] * len(args),
-            out_specs=(any_spec,) * 4,
+            out_specs=(pl.BlockSpec(memory_space=pltpu.VMEM),) * 4,
             scratch_shapes=scratch,
             compiler_params=pltpu.CompilerParams(
-                collective_id=0, has_side_effects=True, vmem_limit_bytes=60 * 1024 * 1024),
+                collective_id=0, has_side_effects=True, vmem_limit_bytes=room),
         )(*args)
+        keys, vals, rope, att = pl.pallas_call(
+            put_out,
+            out_shape=tuple(jax.ShapeDtypeStruct(shape, BF16) for shape in shapes),
+            in_specs=[pl.BlockSpec(memory_space=pltpu.VMEM)] * 4,
+            out_specs=(any_spec,) * 4,
+            scratch_shapes=[dma((4,))],
+            compiler_params=pltpu.CompilerParams(vmem_limit_bytes=4 * 1024 * 1024),
+        )(*made)
         return (
             keys.reshape(1, fresh, hk),
             vals.reshape(1, fresh, hv),

time: 32.4 us -> 26.6 us (0.82)
  local copies, waits for them, and re-layouts: 5.78 us -> 0 us
    unnamed x4 -> x0, local copies, waits for them, and re-layouts: 5.78 us -> none
    pallas_call x1 -> x2, Pallas kernels: 25.7 us -> 25.8 us  [the longest x1 25.1 us: on_device(): pl.pallas_call(functools.partial(kernel, cfg), out_shape=tuple((pltpu.VME...]
where the time goes in v2:
time: 26.6 us; the launch traced here: 26.5 us
  Pallas kernels  25.8 us (97%)
  between operations  0.64 us (2%)
    pallas_call x1, Pallas kernels, on_device(): pl.pallas_call(functools.partial(kernel, cfg), out_shape=tuple((pltpu.VME...  25.1 us
    pallas_call x1, Pallas kernels, on_device(): pl.pallas_call(put_out, out_shape=tuple((jax.ShapeDtypeStruct(shape, BF16...  0.76 us

profile of v2, /device:TPU:0, one launch (start us, length us, event | category | flops | bytes accessed | tf_op | source)
XLA Modules:
  0.0 26.5 jit_solution(16473226841850230474)
XLA Ops:
  0.6 25.1 %shard_map.165 = (bf16[80,1024]{1,0:T(8,128)(2,1)S(1)}, bf16[80,1024]{1,0:T(8,128)(2,1)S(1)}, bf16[64,80]{1,0:T(8,128)(2,1)S(1)}, bf16[1,1024]{1,0:T(2,128)(2,1)S(1)}) custom-call(bf16[80,1024]{1,0:T(8,128)(2,1)} %bitcast.17, bf16[4096,512]{1,0:T(8,128)(2,1)} %refs_1_.1, bf16[64,4096]{1,0:T(8,128)(2,1)} %bitcast.16, f32[1,512]{1,0:T(1,128)} %bitcast.18, ...), custom_call_target="tpu_custom_call" | custom-call | tf_op jit(solution)/shard_map/pallas_call | solution.py:333
  25.7 0.8 %shard_map.166 = (bf16[80,1024]{1,0:T(8,128)(2,1)}, bf16[80,1024]{1,0:T(8,128)(2,1)}, bf16[64,80]{1,0:T(8,128)(2,1)}, bf16[1,1024]{1,0:T(2,128)(2,1)}) custom-call(bf16[80,1024]{1,0:T(8,128)(2,1)S(1)} %get-tuple-element.12.refs_0_, bf16[80,1024]{1,0:T(8,128)(2,1)S(1)} %get-tuple-element.13.refs_1_, bf16[64,80]{1,0:T(8,128)(2,1)S(1)} %get-tuple-element.14.refs_2_, ...), custom_call_target="tpu_custom_call" | custom-call | tf_op jit(solution)/shard_map/pallas_call | solution.py:342

commit v3 on v2

--- a/solution.py
+++ b/solution.py
@@ -136,55 +136,58 @@
     q_all_lat = q_all[:, :lw].astype(BF16)
     q_all_rot = q_all[:, lw:lw + ROPE].astype(BF16)
     copies["prope"].wait()
+    def row_copy(k, d):
+        return pltpu.make_async_remote_copy(
+            src_ref=lat_send.at[k], dst_ref=lat_recv.at[s],
+            send_sem=l_ss.at[k * ntp + d], recv_sem=l_rs.at[s],
+            device_id=(k * ntp + t, lax.rem(t + d, ntp)), device_id_type=MESH)
+
+    def pass_rows():
+        total = part_send[t]
+        for d in range(1, ntp):
+            peer = lax.rem(t + d, ntp)
+            peer_copy(part_recv.at[peer], part_recv.at[peer], p_ss.at[d], p_rs.at[peer], peer).wait_recv()
+            total = total + part_recv[peer]
+        copies["gain"].wait()
+        copies["table"].wait()
+        raw = total[:, :lw]
+        scale = lax.rsqrt(jnp.mean(raw * raw, axis=-1, keepdims=True) + epsilon)
+        latent = raw * scale * gain[...]
+        turn = total[:, lw:lw + ROPE]
+        half = ROPE // 2
+        swapped = jnp.concatenate([turn[:, half:], turn[:, :half]], axis=1)
+        turned = turn * table[:, :ROPE] + swapped * table[:, ROPE:]
+        both = jnp.concatenate([latent, turned, jnp.zeros((gp, LANES - ROPE), F32)], axis=1)
+        for k in range(groups):
+            block = both[k * npos:(k + 1) * npos]
+            if slot > npos:
+                block = jnp.concatenate([block, jnp.zeros((slot - npos, both.shape[1]), F32)], axis=0)
+            lat_send[k] = block.astype(BF16)
+
+        for k in range(groups):
+            for d in range(1, ntp):
+                c = row_copy(k, d)
+                c.start()
+                pending.append(c)
+
+            @pl.when(k * ntp + t != s)
+            def _():
+                row_copy(k, 0).start()
+
+            @pl.when(k * ntp + t == s)
+            def _():
+                lat_recv[s] = lat_send[k]
+
     high = None
     for c in range(chunks):
+        if c == chunks // 2:
+            pass_rows()
         cache_copies[c].wait()
         cols = slice(c * chunk, (c + 1) * chunk)
         sc = (dot(q_all_lat, cache[cols, :], 1, 1) + dot(q_all_rot, prope[:, cols], 1, 0)) * factor
         scores[:, cols] = sc
         top = jnp.max(sc, axis=1, keepdims=True)
         high = top if high is None else jnp.maximum(high, top)
-
-    total = part_send[t]
-    for d in range(1, ntp):
-        peer = lax.rem(t + d, ntp)
-        peer_copy(part_recv.at[peer], part_recv.at[peer], p_ss.at[d], p_rs.at[peer], peer).wait_recv()
-        total = total + part_recv[peer]
-    copies["gain"].wait()
-    copies["table"].wait()
-    raw = total[:, :lw]
-    scale = lax.rsqrt(jnp.mean(raw * raw, axis=-1, keepdims=True) + epsilon)
-    latent = raw * scale * gain[...]
-    turn = total[:, lw:lw + ROPE]
-    half = ROPE // 2
-    swapped = jnp.concatenate([turn[:, half:], turn[:, :half]], axis=1)
-    turned = turn * table[:, :ROPE] + swapped * table[:, ROPE:]
-    both = jnp.concatenate([latent, turned, jnp.zeros((gp, LANES - ROPE), F32)], axis=1)
-    for k in range(groups):
-        block = both[k * npos:(k + 1) * npos]
-        if slot > npos:
-            block = jnp.concatenate([block, jnp.zeros((slot - npos, both.shape[1]), F32)], axis=0)
-        lat_send[k] = block.astype(BF16)
-
-    def row_copy(k, d):
-        return pltpu.make_async_remote_copy(
-            src_ref=lat_send.at[k], dst_ref=lat_recv.at[s],
-            send_sem=l_ss.at[k * ntp + d], recv_sem=l_rs.at[s],
-            device_id=(k * ntp + t, lax.rem(t + d, ntp)), device_id_type=MESH)
-
-    for k in range(groups):
-        for d in range(1, ntp):
-            c = row_copy(k, d)
-            c.start()
-            pending.append(c)
-
-        @pl.when(k * ntp + t != s)
-        def _():
-            row_copy(k, 0).start()
-
-        @pl.when(k * ntp + t == s)
-        def _():
-            lat_recv[s] = lat_send[k]
 
     summed = None
     mass = None

time: 26.6 us -> 23.5 us (0.88)
  Pallas kernels: 25.8 us -> 22.7 us
    pallas_call x1, Pallas kernels: 25.1 us -> 21.9 us  [on_device(): pl.pallas_call(functools.partial(kernel, cfg), out_shape=tuple((pltpu.VME...]
where the time goes in v3:
time: 23.5 us; the launch traced here: 23.3 us
  Pallas kernels  22.7 us (97%)
  between operations  0.64 us (3%)
    pallas_call x1, Pallas kernels, on_device(): pl.pallas_call(functools.partial(kernel, cfg), out_shape=tuple((pltpu.VME...  21.9 us
    pallas_call x1, Pallas kernels, on_device(): pl.pallas_call(put_out, out_shape=tuple((jax.ShapeDtypeStruct(shape, BF16...  0.76 us

profile of v3, /device:TPU:0, one launch (start us, length us, event | category | flops | bytes accessed | tf_op | source)
XLA Modules:
  0.0 23.3 jit_solution(2560348489190866409)
XLA Ops:
  0.6 21.9 %shard_map.165 = (bf16[80,1024]{1,0:T(8,128)(2,1)S(1)}, bf16[80,1024]{1,0:T(8,128)(2,1)S(1)}, bf16[64,80]{1,0:T(8,128)(2,1)S(1)}, bf16[1,1024]{1,0:T(2,128)(2,1)S(1)}) custom-call(bf16[80,1024]{1,0:T(8,128)(2,1)} %bitcast.17, bf16[4096,512]{1,0:T(8,128)(2,1)} %refs_1_.1, bf16[64,4096]{1,0:T(8,128)(2,1)} %bitcast.16, f32[1,512]{1,0:T(1,128)} %bitcast.18, ...), custom_call_target="tpu_custom_call" | custom-call | tf_op jit(solution)/shard_map/pallas_call | solution.py:336
  22.6 0.8 %shard_map.166 = (bf16[80,1024]{1,0:T(8,128)(2,1)}, bf16[80,1024]{1,0:T(8,128)(2,1)}, bf16[64,80]{1,0:T(8,128)(2,1)}, bf16[1,1024]{1,0:T(2,128)(2,1)}) custom-call(bf16[80,1024]{1,0:T(8,128)(2,1)S(1)} %get-tuple-element.12.refs_0_, bf16[80,1024]{1,0:T(8,128)(2,1)S(1)} %get-tuple-element.13.refs_1_, bf16[64,80]{1,0:T(8,128)(2,1)S(1)} %get-tuple-element.14.refs_2_, ...), custom_call_target="tpu_custom_call" | custom-call | tf_op jit(solution)/shard_map/pallas_call | solution.py:345

commit v4 on v3

--- a/solution.py
+++ b/solution.py
@@ -180,7 +180,7 @@
 
     high = None
     for c in range(chunks):
-        if c == chunks // 2:
+        if c == chunks // 4:
             pass_rows()
         cache_copies[c].wait()
         cols = slice(c * chunk, (c + 1) * chunk)

time: 23.5 us -> 22.4 us (0.953)
  Pallas kernels: 22.7 us -> 21.6 us
    pallas_call x1, Pallas kernels: 21.9 us -> 20.8 us  [on_device(): pl.pallas_call(functools.partial(kernel, cfg), out_shape=tuple((pltpu.VME...]
where the time goes in v4:
time: 22.4 us; the launch traced here: 22.2 us
  Pallas kernels  21.6 us (96%)
  between operations  0.64 us (3%)
    pallas_call x1, Pallas kernels, on_device(): pl.pallas_call(functools.partial(kernel, cfg), out_shape=tuple((pltpu.VME...  20.8 us
    pallas_call x1, Pallas kernels, on_device(): pl.pallas_call(put_out, out_shape=tuple((jax.ShapeDtypeStruct(shape, BF16...  0.76 us

profile of v4, /device:TPU:0, one launch (start us, length us, event | category | flops | bytes accessed | tf_op | source)
XLA Modules:
  0.0 22.2 jit_solution(6869160262871759857)
XLA Ops:
  0.6 20.8 %shard_map.165 = (bf16[80,1024]{1,0:T(8,128)(2,1)S(1)}, bf16[80,1024]{1,0:T(8,128)(2,1)S(1)}, bf16[64,80]{1,0:T(8,128)(2,1)S(1)}, bf16[1,1024]{1,0:T(2,128)(2,1)S(1)}) custom-call(bf16[80,1024]{1,0:T(8,128)(2,1)} %bitcast.17, bf16[4096,512]{1,0:T(8,128)(2,1)} %refs_1_.1, bf16[64,4096]{1,0:T(8,128)(2,1)} %bitcast.16, f32[1,512]{1,0:T(1,128)} %bitcast.18, ...), custom_call_target="tpu_custom_call" | custom-call | tf_op jit(solution)/shard_map/pallas_call | solution.py:336
  21.5 0.8 %shard_map.166 = (bf16[80,1024]{1,0:T(8,128)(2,1)}, bf16[80,1024]{1,0:T(8,128)(2,1)}, bf16[64,80]{1,0:T(8,128)(2,1)}, bf16[1,1024]{1,0:T(2,128)(2,1)}) custom-call(bf16[80,1024]{1,0:T(8,128)(2,1)S(1)} %get-tuple-element.12.refs_0_, bf16[80,1024]{1,0:T(8,128)(2,1)S(1)} %get-tuple-element.13.refs_1_, bf16[64,80]{1,0:T(8,128)(2,1)S(1)} %get-tuple-element.14.refs_2_, ...), custom_call_target="tpu_custom_call" | custom-call | tf_op jit(solution)/shard_map/pallas_call | solution.py:345

commit v5 on v4

--- a/solution.py
+++ b/solution.py
@@ -99,21 +99,6 @@
     q_send[...] = q_own
     q_recv[t] = q_own
 
-    self_row = from_t == t
-    pl.semaphore_wait(
-        barrier, ntp - 1 + ntp * groups - ntp * jnp.where(self_row, 1, 0).astype(jnp.int32))
-
-    def peer_copy(src, dst, ssem, rsem, peer):
-        return pltpu.make_async_remote_copy(
-            src_ref=src, dst_ref=dst, send_sem=ssem, recv_sem=rsem,
-            device_id=(s, peer), device_id_type=MESH)
-
-    pending = []
-    for d in range(1, ntp):
-        c = peer_copy(q_send, q_recv.at[t], q_ss.at[d], q_rs.at[t], lax.rem(t + d, ntp))
-        c.start()
-        pending.append(c)
-
     for name in ("tok", "perm", "wd", "wr"):
         copies[name].wait()
     rows = dot(perm[...], tok[...], 1, 0).astype(BF16)
@@ -123,6 +108,20 @@
         part_send[u, :, :lw] = lat_part[u * gp:(u + 1) * gp]
         part_send[u, :, lw:lw + ROPE] = rope_part[u * gp:(u + 1) * gp]
         part_send[u, :, lw + ROPE:] = jnp.zeros((gp, LANES - ROPE), F32)
+    self_row = from_t == t
+    pl.semaphore_wait(
+        barrier, ntp - 1 + ntp * groups - ntp * jnp.where(self_row, 1, 0).astype(jnp.int32))
+
+    def peer_copy(src, dst, ssem, rsem, peer):
+        return pltpu.make_async_remote_copy(
+            src_ref=src, dst_ref=dst, send_sem=ssem, recv_sem=rsem,
+            device_id=(s, peer), device_id_type=MESH)
+
+    pending = []
+    for d in range(1, ntp):
+        c = peer_copy(q_send, q_recv.at[t], q_ss.at[d], q_rs.at[t], lax.rem(t + d, ntp))
+        c.start()
+        pending.append(c)
     for d in range(1, ntp):
         peer = lax.rem(t + d, ntp)
         c = peer_copy(part_send.at[peer], part_recv.at[t], p_ss.at[d], p_rs.at[t], peer)
@@ -180,7 +179,7 @@
 
     high = None
     for c in range(chunks):
-        if c == chunks // 4:
+        if c == chunks // 8:
             pass_rows()
         cache_copies[c].wait()
         cols = slice(c * chunk, (c + 1) * chunk)

time: 22.4 us -> 23.2 us (1.036)
  Pallas kernels: 21.6 us -> 22.4 us
    pallas_call x1, Pallas kernels: 20.8 us -> 21.6 us  [on_device(): pl.pallas_call(functools.partial(kernel, cfg), out_shape=tuple((pltpu.VME...]
where the time goes in v5:
time: 23.2 us; the launch traced here: 23 us
  Pallas kernels  22.4 us (97%)
  between operations  0.64 us (3%)
    pallas_call x1, Pallas kernels, on_device(): pl.pallas_call(functools.partial(kernel, cfg), out_shape=tuple((pltpu.VME...  21.6 us
    pallas_call x1, Pallas kernels, on_device(): pl.pallas_call(put_out, out_shape=tuple((jax.ShapeDtypeStruct(shape, BF16...  0.76 us

profile of v5, /device:TPU:0, one launch (start us, length us, event | category | flops | bytes accessed | tf_op | source)
XLA Modules:
  0.0 23.0 jit_solution(2391014063154557783)
XLA Ops:
  0.6 21.6 %shard_map.165 = (bf16[80,1024]{1,0:T(8,128)(2,1)S(1)}, bf16[80,1024]{1,0:T(8,128)(2,1)S(1)}, bf16[64,80]{1,0:T(8,128)(2,1)S(1)}, bf16[1,1024]{1,0:T(2,128)(2,1)S(1)}) custom-call(bf16[80,1024]{1,0:T(8,128)(2,1)} %bitcast.17, bf16[4096,512]{1,0:T(8,128)(2,1)} %refs_1_.1, bf16[64,4096]{1,0:T(8,128)(2,1)} %bitcast.16, f32[1,512]{1,0:T(1,128)} %bitcast.18, ...), custom_call_target="tpu_custom_call" | custom-call | tf_op jit(solution)/shard_map/pallas_call | solution.py:335
  22.3 0.8 %shard_map.166 = (bf16[80,1024]{1,0:T(8,128)(2,1)}, bf16[80,1024]{1,0:T(8,128)(2,1)}, bf16[64,80]{1,0:T(8,128)(2,1)}, bf16[1,1024]{1,0:T(2,128)(2,1)}) custom-call(bf16[80,1024]{1,0:T(8,128)(2,1)S(1)} %get-tuple-element.12.refs_0_, bf16[80,1024]{1,0:T(8,128)(2,1)S(1)} %get-tuple-element.13.refs_1_, bf16[64,80]{1,0:T(8,128)(2,1)S(1)} %get-tuple-element.14.refs_2_, ...), custom_call_target="tpu_custom_call" | custom-call | tf_op jit(solution)/shard_map/pallas_call | solution.py:344

commit v6 on v4

--- a/solution.py
+++ b/solution.py
@@ -69,6 +69,18 @@
     load("gain", gain_h, gain)
     load("table", table_h.at[s], table)
     load("sel", sel_h, sel)
+
+    barrier = pltpu.get_barrier_semaphore()
+    for d in range(1, ntp):
+        pl.semaphore_signal(barrier, inc=1, device_id=(s, lax.rem(t + d, ntp)), device_id_type=MESH)
+    from_t = lax.rem(s, ntp)
+    for src in range(nsp):
+        @pl.when(src != s)
+        def _():
+            pl.semaphore_signal(barrier, inc=1, device_id=(src, from_t), device_id_type=MESH)
+
+    for name in ("qn", "qr", "ku", "fold", "tok", "perm", "wd", "wr"):
+        copies[name].wait()
     load("prope", prope_h, prope)
     cache_copies = []
     for c in range(chunks):
@@ -77,18 +89,6 @@
         cc.start()
         cache_copies.append(cc)
     load("vu", vu_h, vu)
-
-    barrier = pltpu.get_barrier_semaphore()
-    for d in range(1, ntp):
-        pl.semaphore_signal(barrier, inc=1, device_id=(s, lax.rem(t + d, ntp)), device_id_type=MESH)
-    from_t = lax.rem(s, ntp)
-    for src in range(nsp):
-        @pl.when(src != s)
-        def _():
-            pl.semaphore_signal(barrier, inc=1, device_id=(src, from_t), device_id_type=MESH)
-
-    for name in ("qn", "qr", "ku", "fold"):
-        copies[name].wait()
     qn_row = jnp.broadcast_to(qn[...].astype(F32), (heads, qn.shape[1]))
     q_bd = jnp.where(head_mask(qn_row.shape, PLAIN_KEY_WIDTH), qn_row, 0.0).astype(BF16)
     qr_row = jnp.broadcast_to(qr[...].astype(F32), (heads, qr.shape[1]))
@@ -114,8 +114,6 @@
         c.start()
         pending.append(c)
 
-    for name in ("tok", "perm", "wd", "wr"):
-        copies[name].wait()
     rows = dot(perm[...], tok[...], 1, 0).astype(BF16)
     lat_part = dot(rows, wd[...], 1, 0)
     rope_part = dot(rows, wr[...], 1, 1)

time: 22.4 us -> 22.4 us (level)
  no operation moved by 1% of the time
where the time goes in v6:
time: 22.4 us; the launch traced here: 22.2 us
  Pallas kernels  21.6 us (96%)
  between operations  0.64 us (3%)
    pallas_call x1, Pallas kernels, on_device(): pl.pallas_call(functools.partial(kernel, cfg), out_shape=tuple((pltpu.VME...  20.8 us
    pallas_call x1, Pallas kernels, on_device(): pl.pallas_call(put_out, out_shape=tuple((jax.ShapeDtypeStruct(shape, BF16...  0.76 us

profile of v6, /device:TPU:0, one launch (start us, length us, event | category | flops | bytes accessed | tf_op | source)
XLA Modules:
  0.0 22.2 jit_solution(214774966207508130)
XLA Ops:
  0.6 20.8 %shard_map.165 = (bf16[80,1024]{1,0:T(8,128)(2,1)S(1)}, bf16[80,1024]{1,0:T(8,128)(2,1)S(1)}, bf16[64,80]{1,0:T(8,128)(2,1)S(1)}, bf16[1,1024]{1,0:T(2,128)(2,1)S(1)}) custom-call(bf16[80,1024]{1,0:T(8,128)(2,1)} %bitcast.17, bf16[4096,512]{1,0:T(8,128)(2,1)} %refs_1_.1, bf16[64,4096]{1,0:T(8,128)(2,1)} %bitcast.16, f32[1,512]{1,0:T(1,128)} %bitcast.18, ...), custom_call_target="tpu_custom_call" | custom-call | tf_op jit(solution)/shard_map/pallas_call | solution.py:334
  21.5 0.8 %shard_map.166 = (bf16[80,1024]{1,0:T(8,128)(2,1)}, bf16[80,1024]{1,0:T(8,128)(2,1)}, bf16[64,80]{1,0:T(8,128)(2,1)}, bf16[1,1024]{1,0:T(2,128)(2,1)}) custom-call(bf16[80,1024]{1,0:T(8,128)(2,1)S(1)} %get-tuple-element.12.refs_0_, bf16[80,1024]{1,0:T(8,128)(2,1)S(1)} %get-tuple-element.13.refs_1_, bf16[64,80]{1,0:T(8,128)(2,1)S(1)} %get-tuple-element.14.refs_2_, ...), custom_call_target="tpu_custom_call" | custom-call | tf_op jit(solution)/shard_map/pallas_call | solution.py:343
